TPU v7x, 32 devices: a whole 2x2x4 slice. The times are simulated.
32 devices in a mesh: dp: 4 (over y, x), kv: 4 (over z), tp: 2 (over core).
Axes of the slice: x: 2, y: 2, z: 4, core: 2. Of those that a mesh axis runs over, the one named last changes fastest.
Arguments:
- tokens: bfloat16 [4, 1280, 2048], P('dp', 'kv'), may hold values from -72 to 72
- w_query: bfloat16 [2048, 512], P(None, 'tp'), may hold values from -0.125 to 0.125
- key_weight: bfloat16 [2048, 256], P(None, 'tp'), may hold values from -0.125 to 0.125
- value_weight: bfloat16 [2048, 256], P(None, 'tp'), may hold values from -2.09375 to 2.09375
- w_out: bfloat16 [512, 2048], P(None, 'tp'), may hold values from -0.25 to 0.25
- chosen: int32 [4, 40, 16], P('dp', 'kv'), may hold values from -1 to 39, as said below
Outputs:
- mixed: bfloat16 [4, 1280, 2048], P('dp', 'kv', 'tp')
- log_mass: float32 [4, 4, 1280], P('dp', 'tp', 'kv')
Inputs may be any that keep to these rules, and one draw needn't show every extreme that they name: `chosen`: entry 0 of row i of a sequence is i; the other entries are distinct blocks before i, or -1 for an empty slot. The 10 rows of one index of kv together name at most one block held by any other index of kv; this bound is reached.
All inputs are finite; a program needn't handle non-finite values.
Results may differ from a plain program's by a relative error of at most 0.006.
The roundings to bfloat16 on the way count: a program that leaves them out, or rounds other values in their place, can miss the bound.
Values may be sent and summed in bfloat16 or wider, within the bound.
No kernel may reach another device: no remote copies, remote signals or barrier semaphores. Data moves between devices by JAX's collectives and lax.ppermute only.
A program may use at most 64 MiB of HBM per device.

v0:
```python
import jax
import jax.numpy as jnp
from jax import lax
from jax.sharding import PartitionSpec as P

HEAD_WIDTH = 128


def body(tokens, w_query, key_weight, value_weight, w_out, chosen):
    local_tokens = tokens[0]
    local_chosen = chosen[0]
    row_count = local_tokens.shape[0]
    blocks_here, select_count = local_chosen.shape
    block_rows = row_count // blocks_here
    kv_heads = key_weight.shape[1] // HEAD_WIDTH
    query_heads = w_query.shape[1] // HEAD_WIDTH
    heads_per_group = query_heads // kv_heads
    width_kv = kv_heads * HEAD_WIDTH
    devices = lax.axis_size("kv")
    my_index = lax.axis_index("kv")
    queries = jnp.dot(local_tokens, w_query, preferred_element_type=jnp.float32).astype(
        jnp.bfloat16
    )
    projected_keys = jnp.dot(local_tokens, key_weight, preferred_element_type=jnp.float32).astype(
        jnp.bfloat16
    )
    projected_values = jnp.dot(
        local_tokens, value_weight, preferred_element_type=jnp.float32
    ).astype(jnp.bfloat16)
    paired = jnp.concatenate([projected_keys, projected_values], axis=1)
    gathered = lax.all_gather(paired, "kv", axis=0, tiled=True)
    block_table = gathered.reshape(devices * blocks_here, block_rows, 2 * width_kv)
    lookup = jnp.maximum(local_chosen, 0)
    picked = jnp.take(block_table, lookup, axis=0)
    selected_keys = picked[..., :width_kv].reshape(
        blocks_here, select_count * block_rows, kv_heads, HEAD_WIDTH
    )
    selected_values = picked[..., width_kv:].reshape(
        blocks_here, select_count * block_rows, kv_heads, HEAD_WIDTH
    )
    grouped_queries = queries.reshape(
        blocks_here, block_rows, kv_heads, heads_per_group, HEAD_WIDTH
    )
    scores = jnp.einsum(
        "btkgd,bskd->bkgts", grouped_queries, selected_keys, preferred_element_type=jnp.float32
    ) * HEAD_WIDTH ** (-0.5)
    bounded_index = jnp.maximum(local_chosen, 0)
    key_pos = (
        bounded_index[..., None] * block_rows + jnp.arange(block_rows, dtype=jnp.int32)
    ).reshape(blocks_here, select_count * block_rows)
    key_live = jnp.repeat(local_chosen >= 0, block_rows, axis=1)
    block_ids = my_index * blocks_here + jnp.arange(blocks_here, dtype=jnp.int32)
    query_pos = block_ids[:, None] * block_rows + jnp.arange(block_rows, dtype=jnp.int32)[None, :]
    allowed = key_live[:, None, :] & (key_pos[:, None, :] <= query_pos[:, :, None])
    scores = jnp.where(allowed[:, None, None], scores, -jnp.inf)
    row_max = jnp.max(scores, axis=-1)
    weights = jnp.exp(scores - row_max[..., None])
    row_sum = jnp.sum(weights, axis=-1)
    probs_low = weights.astype(jnp.bfloat16)
    summed = jnp.einsum(
        "bkgts,bskd->btkgd", probs_low, selected_values, preferred_element_type=jnp.float32
    )
    attended = (
        (summed / row_sum.transpose(0, 3, 1, 2)[..., None])
        .astype(jnp.bfloat16)
        .reshape(row_count, query_heads * HEAD_WIDTH)
    )
    log_mass = (row_max + jnp.log(row_sum)).transpose(1, 2, 0, 3).reshape(query_heads, row_count)
    mixed = jnp.dot(
        lax.all_gather(attended, "tp", axis=1, tiled=True),
        w_out,
        preferred_element_type=jnp.float32,
    ).astype(jnp.bfloat16)
    return (mixed[None], log_mass[None])


def solution(mesh):
    in_specs = (
        P("dp", "kv", None),
        P(None, "tp"),
        P(None, "tp"),
        P(None, "tp"),
        P(None, "tp"),
        P("dp", "kv", None),
    )
    out_specs = (P("dp", "kv", "tp"), P("dp", "tp", "kv"))
    return jax.shard_map(body, mesh=mesh, in_specs=in_specs, out_specs=out_specs, check_vma=False)
```

profile of v0, /device:TPU:0, one launch (start us, length us, event | category | flops | bytes accessed | tf_op | source)
XLA Modules:
  0.0 39.9 jit_solution(1609023411895982091)
XLA Ops:
  0.6 0.0 copy-start
  0.6 0.0 copy-start.3
  0.7 0.8 %broadcast_compare_fusion.1 = (pred[1,10,16]{2,0,1:T(4,128)(4,1)S(1)}, pred[1,10,16]{2,0,1:T(4,128)(4,1)S(1)}) fusion(s32[1,10,16]{2,0,1:T(1,128)} %param.11), kind=kLoop, calls=%fused_computation.39 | loop fusion | flops 480 | bytes 960 | tf_op jit(solution)/shard_map/ge | solution.py:51
  1.5 0.7 %broadcast_multiply_fusion = (s32[1,10,16]{2,0,1:T(1,128)S(1)}, s32[10,16]{1,0:T(8,128)S(1)}) fusion(s32[1,10,16]{2,0,1:T(1,128)} %param.11), kind=kLoop, calls=%fused_computation.37 | loop fusion | flops 320 | bytes 1920 | tf_op jit(solution)/shard_map/mul | solution.py:49
  2.2 0.1 reshape.141
  2.3 0.0 copy-done
  2.3 1.6 %fusion.14 = bf16[320,128]{1,0:T(8,128)(2,1)S(1)} fusion(bf16[2048,128]{1,0:T(8,128)(2,1)} %param.8, bf16[1,320,2048]{2,1,0:T(8,128)(2,1)S(1)} %copy-done), kind=kOutput, calls=%fused_computation.18 | convolution fusion | flops 167813120 | bytes 1916928 | tf_op jit(solution)/shard_map/dot_general | solution.py:24
  3.9 0.0 copy-done.3
  3.9 0.5 %fusion.17 = bf16[320,128]{1,0:T(8,128)(2,1)S(1)} fusion(bf16[2048,128]{1,0:T(8,128)(2,1)S(1)} %copy-done.3, bf16[1,320,2048]{2,1,0:T(8,128)(2,1)S(1)} %copy-done), kind=kOutput, calls=%fused_computation.19 | convolution fusion | flops 167813120 | bytes 1916928 | tf_op jit(solution)/shard_map/dot_general | solution.py:27
  4.4 19.7 %all_gather.6 = bf16[1280,256]{1,0:T(8,128)(2,1)S(1)} all-gather(bf16[320,256]{1,0:T(8,128)(2,1)S(1)} %pad_maximum_fusion), channel_id=1, replica_groups=mesh['dp'=4,'kv'=4,'tp'=2] {'kv'}, dimensions={0}, use_global_device_ids=true | all-gather | bytes 819200 | tf_op jit(solution)/shard_map/all_gather | solution.py:31
  24.2 2.5 %gather_fusion = bf16[160,32,256]{2,1,0:T(8,128)(2,1)} fusion(bf16[40,32,256]{2,1,0:T(8,128)(2,1)S(1)} %bitcast.78, s32[1024]{0:T(1024)S(1)} %pad_clamp_fusion), kind=kCustom, calls=%fused_computation | custom fusion | bytes 5243520 | tf_op jit(solution)/shard_map/jit(_take)/gather | solution.py:34
  26.7 2.1 %broadcast_select_fusion = bf16[10,16,32,256]{3,2,1,0:T(8,128)(2,1)S(1)} fusion(bf16[10,16,32,256]{3,2,1,0:T(8,128)(2,1)} %bitcast.79, pred[10,16]{1,0:T(8,128)(4,1)S(1)} %get-tuple-element.11), kind=kLoop, calls=%fused_computation.1 | loop fusion | flops 1310720 | bytes 5243040 | tf_op jit(solution)/shard_map/jit(_take)/select_n | solution.py:34
  28.7 1.8 %fusion.28 = (bf16[10,16,32,128]{3,2,1,0:T(8,128)(2,1)S(1)}, bf16[10,16,32,128]{3,2,1,0:T(8,128)(2,1)}) fusion(bf16[10,16,32,256]{3,2,1,0:T(8,128)(2,1)S(1)} %broadcast_select_fusion), kind=kLoop, calls=%fused_computation.43 | loop fusion | bytes 5242880 | tf_op jit(solution)/shard_map/slice | solution.py:35
  30.5 0.1 broadcast_in_dim.38
  30.6 0.1 and.20
  30.7 0.1 add.65
  30.8 0.1 add.66
  30.9 0.1 add.68
  31.0 0.1 iota_add_fusion
  31.1 0.2 compare_and_fusion
  31.3 1.7 %fusion.9 = bf16[320,256]{1,0:T(8,128)(2,1)S(1)} fusion(bf16[2048,256]{1,0:T(8,128)(2,1)} %param.7, bf16[1,320,2048]{2,1,0:T(8,128)(2,1)S(1)} %copy-done), kind=kOutput, calls=%fused_computation.15 | convolution fusion | flops 335626240 | bytes 2523136 | tf_op jit(solution)/shard_map/dot_general | solution.py:21
  33.0 0.7 %fusion.29 = (f32[10,2,32]{2,1,0:T(2,128)S(1)}, f32[10,1,2,32,512]{4,3,2,0,1:T(8,128)S(1)}) fusion(bf16[10,512,128,1]{2,1,3,0:T(8,128)(2,1)S(1)} %bitcast.80, bf16[10,32,2,128]{3,2,1,0:T(2,128)(2,1)S(1)} %reshape.136, pred[10,32,512]{2,1,0:T(8,128)(4,1)S(1)} %compare_and_fusion), kind=kOutput, calls=%fused_computation.44 | convolution fusion | flops 84868480 | bytes 2951680 | tf_op jit(solution)/shard_map/btkgd,bskd->bkgts/dot_general | solution.py:44
  33.7 0.0 copy-start.1
  33.7 0.5 %fusion.12 = f32[10,2,32]{2,1,0:T(2,128)S(1)} fusion(f32[10,1,2,32,512]{4,3,2,0,1:T(8,128)S(1)} %get-tuple-element.9, f32[10,2,32]{2,1,0:T(2,128)S(1)} %get-tuple-element.8), kind=kLoop, calls=%fused_computation.16 | loop fusion | flops 654720 | bytes 1315840 | tf_op jit(solution)/shard_map/reduce_sum | solution.py:58
  34.2 0.9 %copy-done.1 = bf16[10,16,32,128]{3,2,1,0:T(8,128)(2,1)S(1)} copy-done((bf16[10,16,32,128]{3,2,1,0:T(8,128)(2,1)S(1)}, bf16[10,16,32,128]{3,2,1,0:T(8,128)(2,1)}, u32[]{:S(2)}) %copy-start.1) | copy-done | bytes 1310744
  35.0 0.5 %fusion.21 = bf16[10,32,1,2,128]{4,1,3,0,2:T(8,128)(2,1)S(1)} fusion(bf16[10,512,128,1]{2,1,3,0:T(8,128)(2,1)S(1)} %bitcast.81, f32[10,1,2,32,512]{4,3,2,0,1:T(8,128)S(1)} %get-tuple-element.9, f32[10,2,32]{2,1,0:T(2,128)S(1)} %get-tuple-element.8, f32[10,32,2]{1,2,0:T(2,128)S(1)} %bitcast.84), kind=kOutput, calls=%fused_computation.21 | convolution fusion | flops 84705280 | bytes 2790400 | tf_op jit(solution)/shard_map/bkgts,bskd->btkgd/dot_general | solution.py:60
  35.5 0.0 copy-start.2
  35.5 0.1 copy.15
  35.7 2.2 %all_gather.7 = bf16[320,512]{1,0:T(8,128)(2,1)S(1)} all-gather(bf16[320,256]{1,0:T(8,128)(2,1)S(1)} %bitcast.83), channel_id=1, replica_groups=mesh['dp'=4,'kv'=4,'tp'=2] {'tp'}, dimensions={1}, use_global_device_ids=true | all-gather | bytes 491520 | tf_op jit(solution)/shard_map/all_gather | solution.py:70
  37.9 0.0 copy-done.2
  37.9 1.3 %fusion.8 = bf16[1,320,1024]{2,1,0:T(8,128)(2,1)} fusion(bf16[320,512]{1,0:T(8,128)(2,1)S(1)} %all_gather.7, bf16[512,1024]{1,0:T(8,128)(2,1)S(1)} %copy-done.2), kind=kOutput, calls=%fused_computation.13 | convolution fusion | flops 335872000 | bytes 2031616 | tf_op jit(solution)/shard_map/dot_general | solution.py:69
  39.2 0.7 %broadcast_in_dim_reshape.2 = f32[1,2,320]{2,1,0:T(2,128)} reshape(f32[1,2,10,32]{3,2,1,0:T(8,128)S(1)} %copy.16) | data formatting | bytes 5120 | tf_op jit(solution)/shard_map/broadcast_in_dim;reshape | solution.py:74
  (11 shorter events, 0.1 us)
Async XLA Ops:
  0.6 1.7 %copy-start = (bf16[1,320,2048]{2,1,0:T(8,128)(2,1)S(1)}, bf16[1,320,2048]{2,1,0:T(8,128)(2,1)}, u32[]{:S(2)}) copy-start(bf16[1,320,2048]{2,1,0:T(8,128)(2,1)} %param.6) | copy-start | bytes 3932164
  0.6 3.2 %copy-start.3 = (bf16[2048,128]{1,0:T(8,128)(2,1)S(1)}, bf16[2048,128]{1,0:T(8,128)(2,1)}, u32[]{:S(2)}) copy-start(bf16[2048,128]{1,0:T(8,128)(2,1)} %param.9) | copy-start | bytes 1572868
  33.7 1.3 %copy-start.1 = (bf16[10,16,32,128]{3,2,1,0:T(8,128)(2,1)S(1)}, bf16[10,16,32,128]{3,2,1,0:T(8,128)(2,1)}, u32[]{:S(2)}) copy-start(bf16[10,16,32,128]{3,2,1,0:T(8,128)(2,1)} %get-tuple-element.3) | copy-start | bytes 3932164
  35.5 2.4 %copy-start.2 = (bf16[512,1024]{1,0:T(8,128)(2,1)S(1)}, bf16[512,1024]{1,0:T(8,128)(2,1)}, u32[]{:S(2)}) copy-start(bf16[512,1024]{1,0:T(8,128)(2,1)} %param.10) | copy-start | bytes 3145732
where the time goes:
time: 40.2 us; the launch traced here: 39.9 us
  blocking collectives  21.9 us (54%)
  local copies, waits for them, and re-layouts  6.55 us (16%)
  matrix products  6.27 us (16%)
  other arithmetic  4.39 us (11%)
  between operations  0.81 us (2%)
    all_gather x1, blocking collectives, body(): gathered = lax.all_gather(paired, 'kv', axis=0, tiled=True)  19.7 us
    gather x1, local copies, waits for them, and re-layouts, body(): picked = jnp.take(block_table, lookup, axis=0)  2.49 us
    all_gather x1, blocking collectives, body(): lax.all_gather(attended, 'tp', axis=1, tiled=True)  2.17 us
    select_n x1, other arithmetic, body(): picked = jnp.take(block_table, lookup, axis=0)  2.05 us
    slice x1, local copies, waits for them, and re-layouts, body(): picked[..., :width_kv]  1.77 us
    dot_general x1, matrix products, body(): jnp.dot(local_tokens, w_query, preferred_element_type=jnp.float32)  1.73 us
    dot_general x1, matrix products, body(): jnp.dot(local_tokens, key_weight, preferred_element_type=jnp.float32)  1.55 us
    dot_general x1, matrix products, body(): jnp.dot(lax.all_gather(attended, 'tp', axis=1, tiled=True), w_out, prefer...  1.35 us

commit v1 on v0

--- a/solution.py
+++ b/solution.py
@@ -28,7 +28,12 @@
         local_tokens, value_weight, preferred_element_type=jnp.float32
     ).astype(jnp.bfloat16)
     paired = jnp.concatenate([projected_keys, projected_values], axis=1)
-    gathered = lax.all_gather(paired, "kv", axis=0, tiled=True)
+    ring = [paired]
+    for hop in range(3):
+        ring.append(lax.ppermute(ring[-1], "kv", [(dev, (dev + 1) % 4) for dev in range(4)]))
+    gathered = jnp.roll(
+        jnp.concatenate(ring[::-1], axis=0), (lax.axis_index("kv") + 1) * ring[0].shape[0], axis=0
+    )
     block_table = gathered.reshape(devices * blocks_here, block_rows, 2 * width_kv)
     lookup = jnp.maximum(local_chosen, 0)
     picked = jnp.take(block_table, lookup, axis=0)

time: 40.2 us -> 41.7 us (1.037)
  blocking collectives: 21.9 us -> 2.17 us
  waiting for transfers between devices: 0 us -> 18.9 us
  starting transfers between devices: 0 us -> 3.11 us
  other arithmetic: 4.39 us -> 2.89 us
  local copies, waits for them, and re-layouts: 6.55 us -> 6.98 us
    all_gather x1 -> x0, blocking collectives: 19.7 us -> none  [body(): gathered = lax.all_gather(paired, 'kv', axis=0, tiled=True)]
    ppermute x0 -> x3, waiting for transfers between devices: none -> 18.9 us  [body(): lax.ppermute(ring[-1], 'kv', [(dev, (dev + 1) % 4) for dev in range(4)])]
    ppermute x0 -> x3, starting transfers between devices: none -> 3.11 us  [body(): lax.ppermute(ring[-1], 'kv', [(dev, (dev + 1) % 4) for dev in range(4)])]
    dot_general x1, matrix products: 0.46 us -> 1.77 us  [body(): jnp.einsum('bkgts,bskd->btkgd', probs_low, selected_values, preferred_ele...]
    dot_general x1, matrix products: 1.73 us -> 0.52 us  [body(): jnp.dot(local_tokens, w_query, preferred_element_type=jnp.float32)]
    ge x1, other arithmetic: 0.84 us -> 0.02 us  [body(): key_live = jnp.repeat(local_chosen >= 0, block_rows, axis=1)]
    mul x1, other arithmetic: 0.72 us -> 0.02 us  [body(): bounded_index[..., None] * block_rows]
    unnamed x11 -> x19, local copies, waits for them, and re-layouts: 0.92 us -> 1.44 us
  transfers between devices with their start and end apart: 0 -> 3, of which waited for: 0 -> 3; matrix products, arithmetic and copies ran while one was open for 0% -> 3% of each run, Pallas kernels for 0% -> 0%
where the time goes in v1:
time: 41.7 us; the launch traced here: 41.4 us
  waiting for transfers between devices  18.9 us (45%)
  local copies, waits for them, and re-layouts  6.98 us (17%)
  matrix products  6.35 us (15%)
  starting transfers between devices  3.11 us (7%)
  other arithmetic  2.89 us (7%)
  blocking collectives  2.17 us (5%)
  between operations  0.96 us (2%)
    ppermute x3, waiting for transfers between devices, body(): lax.ppermute(ring[-1], 'kv', [(dev, (dev + 1) % 4) for dev in range(4)])  18.9 us
    ppermute x3, starting transfers between devices, body(): lax.ppermute(ring[-1], 'kv', [(dev, (dev + 1) % 4) for dev in range(4)])  3.11 us
    gather x1, local copies, waits for them, and re-layouts, body(): picked = jnp.take(block_table, lookup, axis=0)  2.48 us
    all_gather x1, blocking collectives, body(): lax.all_gather(attended, 'tp', axis=1, tiled=True)  2.17 us
    select_n x1, other arithmetic, body(): picked = jnp.take(block_table, lookup, axis=0)  2.05 us
    dot_general x1, matrix products, body(): jnp.einsum('bkgts,bskd->btkgd', probs_low, selected_values, preferred_ele...  1.77 us
    dot_general x1, matrix products, body(): jnp.dot(local_tokens, key_weight, preferred_element_type=jnp.float32)  1.54 us
    slice x1, local copies, waits for them, and re-layouts, body(): picked[..., :width_kv]  1.53 us
  transfers between devices with their start and end apart: 3, of which 3 were waited for; matrix products, arithmetic and copies ran while one was open for 3% of the time, Pallas kernels for 0%

profile of v1, /device:TPU:0, one launch (start us, length us, event | category | flops | bytes accessed | tf_op | source)
XLA Modules:
  0.0 41.4 jit_solution(8550925106377458723)
XLA Ops:
  0.6 0.0 copy-start
  0.7 1.3 %copy-done = bf16[1,320,2048]{2,1,0:T(8,128)(2,1)S(1)} copy-done((bf16[1,320,2048]{2,1,0:T(8,128)(2,1)S(1)}, bf16[1,320,2048]{2,1,0:T(8,128)(2,1)}, u32[]{:S(2)}) %copy-start) | copy-done | bytes 1310744
  2.0 1.5 %fusion.14 = bf16[320,128]{1,0:T(8,128)(2,1)S(1)} fusion(bf16[2048,128]{1,0:T(8,128)(2,1)} %param.8, bf16[1,320,2048]{2,1,0:T(8,128)(2,1)S(1)} %copy-done), kind=kOutput, calls=%fused_computation.18 | convolution fusion | flops 167813120 | bytes 1916928 | tf_op jit(solution)/shard_map/dot_general | solution.py:24
  3.5 0.0 copy-start.3
  3.5 0.0 copy-start.4
  3.5 0.5 %fusion.17 = bf16[320,128]{1,0:T(8,128)(2,1)S(1)} fusion(bf16[2048,128]{1,0:T(8,128)(2,1)S(1)} %copy-done.2, bf16[1,320,2048]{2,1,0:T(8,128)(2,1)S(1)} %copy-done), kind=kOutput, calls=%fused_computation.19 | convolution fusion | flops 167813120 | bytes 1916928 | tf_op jit(solution)/shard_map/dot_general | solution.py:27
  4.1 3.1 %collective-permute-start = (bf16[320,256]{1,0:T(8,128)(2,1)S(1)}, bf16[320,256]{1,0:T(8,128)(2,1)S(1)}, u32[]{:S(2)}, u32[]{:S(2)}) collective-permute-start(bf16[320,256]{1,0:T(8,128)(2,1)S(1)} %pad_maximum_fusion), channel_id=1, source_target_pairs={{0,2},{2,4},{4,6},{6,0},{1,3},{3,5},{5,7},{7,1},{8,10},{10,12},{12... | collective-permute-start | bytes 491528 | tf_op jit(solution)/shard_map/ppermute | solution.py:33
  7.3 0.1 add.81
  7.3 0.1 add.82
  7.5 0.1 add.84
  7.5 0.5 %fusion.9 = bf16[320,256]{1,0:T(8,128)(2,1)S(1)} fusion(bf16[2048,256]{1,0:T(8,128)(2,1)S(1)} %copy-done.4, bf16[1,320,2048]{2,1,0:T(8,128)(2,1)S(1)} %copy-done), kind=kOutput, calls=%fused_computation.15 | convolution fusion | flops 335626240 | bytes 2523136 | tf_op jit(solution)/shard_map/dot_general | solution.py:21
  8.1 0.1 broadcast_in_dim.38
  8.2 0.1 and.26
  8.3 5.1 %collective-permute-done = bf16[320,256]{1,0:T(8,128)(2,1)S(1)} collective-permute-done((bf16[320,256]{1,0:T(8,128)(2,1)S(1)}, bf16[320,256]{1,0:T(8,128)(2,1)S(1)}, u32[]{:S(2)}, u32[]{:S(2)}) %collective-permute-start) | collective-permute-done | bytes 163872 | tf_op jit(solution)/shard_map/ppermute | solution.py:33
  13.4 0.1 iota_add_fusion
  13.5 7.1 %collective-permute-done.1 = bf16[320,256]{1,0:T(8,128)(2,1)S(1)} collective-permute-done((bf16[320,256]{1,0:T(8,128)(2,1)S(1)}, bf16[320,256]{1,0:T(8,128)(2,1)S(1)}, u32[]{:S(2)}, u32[]{:S(2)}) %collective-permute-start.1) | collective-permute-done | bytes 163872 | tf_op jit(solution)/shard_map/ppermute | solution.py:33
  20.6 0.0 collective-permute-start.2
  20.6 0.2 compare_and_fusion
  20.8 0.1 reshape.141
  21.0 6.7 %collective-permute-done.2 = bf16[320,256]{1,0:T(8,128)(2,1)S(1)} collective-permute-done((bf16[320,256]{1,0:T(8,128)(2,1)S(1)}, bf16[320,256]{1,0:T(8,128)(2,1)S(1)}, u32[]{:S(2)}, u32[]{:S(2)}) %collective-permute-start.2) | collective-permute-done | bytes 163872 | tf_op jit(solution)/shard_map/ppermute | solution.py:33
  27.9 0.2 constant_dynamic-slice_fusion
  28.0 2.5 %gather_fusion = bf16[160,32,256]{2,1,0:T(8,128)(2,1)} fusion(bf16[40,32,256]{2,1,0:T(8,128)(2,1)S(1)} %bitcast.78, s32[1024]{0:T(1024)S(1)} %pad_clamp_fusion), kind=kCustom, calls=%fused_computation | custom fusion | bytes 5243520 | tf_op jit(solution)/shard_map/jit(_take)/gather | solution.py:39
  30.5 2.1 %broadcast_select_fusion = bf16[10,16,32,256]{3,2,1,0:T(8,128)(2,1)S(1)} fusion(bf16[10,16,32,256]{3,2,1,0:T(8,128)(2,1)} %bitcast.79, pred[10,16]{1,0:T(8,128)(4,1)S(1)} %get-tuple-element.11), kind=kLoop, calls=%fused_computation.1 | loop fusion | flops 1310720 | bytes 5243040 | tf_op jit(solution)/shard_map/jit(_take)/select_n | solution.py:39
  32.6 1.5 %fusion.28 = (bf16[10,16,32,128]{3,2,1,0:T(8,128)(2,1)S(1)}, bf16[10,16,32,128]{3,2,1,0:T(8,128)(2,1)}) fusion(bf16[10,16,32,256]{3,2,1,0:T(8,128)(2,1)S(1)} %broadcast_select_fusion), kind=kLoop, calls=%fused_computation.52 | loop fusion | bytes 5242880 | tf_op jit(solution)/shard_map/slice | solution.py:40
  34.1 0.7 %fusion.29 = (f32[10,2,32]{2,1,0:T(2,128)S(1)}, f32[10,1,2,32,512]{4,3,2,0,1:T(8,128)S(1)}) fusion(bf16[10,512,128,1]{2,1,3,0:T(8,128)(2,1)S(1)} %bitcast.80, bf16[10,32,2,128]{3,2,1,0:T(2,128)(2,1)S(1)} %reshape.136, pred[10,32,512]{2,1,0:T(8,128)(4,1)S(1)} %compare_and_fusion), kind=kOutput, calls=%fused_computation.53 | convolution fusion | flops 84868480 | bytes 2951680 | tf_op jit(solution)/shard_map/btkgd,bskd->bkgts/dot_general | solution.py:49
  34.8 0.4 %fusion.12 = f32[10,2,32]{2,1,0:T(2,128)S(1)} fusion(f32[10,1,2,32,512]{4,3,2,0,1:T(8,128)S(1)} %get-tuple-element.9, f32[10,2,32]{2,1,0:T(2,128)S(1)} %get-tuple-element.8), kind=kLoop, calls=%fused_computation.16 | loop fusion | flops 654720 | bytes 1315840 | tf_op jit(solution)/shard_map/reduce_sum | solution.py:63
  35.3 0.7 %broadcast_in_dim_reshape.2 = f32[1,2,320]{2,1,0:T(2,128)} reshape(f32[1,2,10,32]{3,2,1,0:T(8,128)S(1)} %copy.16) | data formatting | bytes 5120 | tf_op jit(solution)/shard_map/broadcast_in_dim;reshape | solution.py:79
  35.9 1.8 %fusion.21 = bf16[10,32,1,2,128]{4,1,3,0,2:T(8,128)(2,1)S(1)} fusion(bf16[10,512,128,1]{2,1,3,0:T(8,128)(2,1)} %bitcast.81, f32[10,1,2,32,512]{4,3,2,0,1:T(8,128)S(1)} %get-tuple-element.9, f32[10,2,32]{2,1,0:T(2,128)S(1)} %get-tuple-element.8, f32[10,32,2]{1,2,0:T(2,128)S(1)} %bitcast.84), kind=kOutput, calls=%fused_computation.21 | convolution fusion | flops 84705280 | bytes 2790400 | tf_op jit(solution)/shard_map/bkgts,bskd->btkgd/dot_general | solution.py:65
  37.7 0.0 copy-start.1
  37.7 0.1 copy.15
  37.9 2.2 %all_gather.3 = bf16[320,512]{1,0:T(8,128)(2,1)S(1)} all-gather(bf16[320,256]{1,0:T(8,128)(2,1)S(1)} %bitcast.83), channel_id=1, replica_groups=mesh['dp'=4,'kv'=4,'tp'=2] {'tp'}, dimensions={1}, use_global_device_ids=true | all-gather | bytes 491520 | tf_op jit(solution)/shard_map/all_gather | solution.py:75
  40.1 1.3 %fusion.8 = bf16[1,320,1024]{2,1,0:T(8,128)(2,1)} fusion(bf16[320,512]{1,0:T(8,128)(2,1)S(1)} %all_gather.3, bf16[512,1024]{1,0:T(8,128)(2,1)S(1)} %copy-done.1), kind=kOutput, calls=%fused_computation.13 | convolution fusion | flops 335872000 | bytes 2031616 | tf_op jit(solution)/shard_map/dot_general | solution.py:74
  (27 shorter events, 0.3 us)
Async XLA Ops:
  0.6 1.3 %copy-start = (bf16[1,320,2048]{2,1,0:T(8,128)(2,1)S(1)}, bf16[1,320,2048]{2,1,0:T(8,128)(2,1)}, u32[]{:S(2)}) copy-start(bf16[1,320,2048]{2,1,0:T(8,128)(2,1)} %param.6) | copy-start | bytes 3932164
  0.6 2.9 %copy-start.2 = (bf16[2048,128]{1,0:T(8,128)(2,1)S(1)}, bf16[2048,128]{1,0:T(8,128)(2,1)}, u32[]{:S(2)}) copy-start(bf16[2048,128]{1,0:T(8,128)(2,1)} %param.9) | copy-start | bytes 1572868
  3.5 3.7 %copy-start.3 = (s32[1,10,16]{2,0,1:T(1,128)S(1)}, s32[1,10,16]{2,0,1:T(1,128)}, u32[]{:S(2)}) copy-start(s32[1,10,16]{2,0,1:T(1,128)} %param.11) | copy-start | bytes 1924
  3.5 4.0 %copy-start.4 = (bf16[2048,256]{1,0:T(8,128)(2,1)S(1)}, bf16[2048,256]{1,0:T(8,128)(2,1)}, u32[]{:S(2)}) copy-start(bf16[2048,256]{1,0:T(8,128)(2,1)} %param.7) | copy-start | bytes 3145732
  4.1 9.3 %collective-permute-start = (bf16[320,256]{1,0:T(8,128)(2,1)S(1)}, bf16[320,256]{1,0:T(8,128)(2,1)S(1)}, u32[]{:S(2)}, u32[]{:S(2)}) collective-permute-start(bf16[320,256]{1,0:T(8,128)(2,1)S(1)} %pad_maximum_fusion), channel_id=1, source_target_pairs={{0,2},{2,4},{4,6},{6,0},{1,3},{3,5},{5,7},{7,1},{8,10},{10,12},{12... | collective-permute-start | bytes 491528 | tf_op jit(solution)/shard_map/ppermute | solution.py:33
  13.4 7.2 %collective-permute-start.1 = (bf16[320,256]{1,0:T(8,128)(2,1)S(1)}, bf16[320,256]{1,0:T(8,128)(2,1)S(1)}, u32[]{:S(2)}, u32[]{:S(2)}) collective-permute-start(bf16[320,256]{1,0:T(8,128)(2,1)S(1)} %collective-permute-done), channel_id=1, source_target_pairs={{0,2},{2,4},{4,6},{6,0},{1,3},{3,5},{5,7},{7,1},{8,10},{10,12},{12... | collective-permute-start | bytes 491528 | tf_op jit(solution)/shard_map/ppermute | solution.py:33
  20.6 7.1 %collective-permute-start.2 = (bf16[320,256]{1,0:T(8,128)(2,1)S(1)}, bf16[320,256]{1,0:T(8,128)(2,1)S(1)}, u32[]{:S(2)}, u32[]{:S(2)}) collective-permute-start(bf16[320,256]{1,0:T(8,128)(2,1)S(1)} %collective-permute-done.1), channel_id=1, source_target_pairs={{0,2},{2,4},{4,6},{6,0},{1,3},{3,5},{5,7},{7,1},{8,10},{10,12},{12... | collective-permute-start | bytes 491528 | tf_op jit(solution)/shard_map/ppermute | solution.py:33
  37.7 2.4 %copy-start.1 = (bf16[512,1024]{1,0:T(8,128)(2,1)S(1)}, bf16[512,1024]{1,0:T(8,128)(2,1)}, u32[]{:S(2)}) copy-start(bf16[512,1024]{1,0:T(8,128)(2,1)} %param.10) | copy-start | bytes 3145732
